TPU v7x, 32 devices: a whole 2x2x4 slice. The times are simulated.
32 devices in a mesh: sp: 4 (over y, x), dp: 8 (over z, core).
Axes of the slice: x: 2, y: 2, z: 4, core: 2. Of those that a mesh axis runs over, the one named last changes fastest.
Arguments:
- tokens: bfloat16 [8, 512, 2048], P('dp', 'sp'), may hold values from -6 to 6
- query_weight: bfloat16 [2048, 1024], P('dp'), may hold values from -0.125 to 0.125
- key_weight: bfloat16 [2048, 1024], P('dp'), may hold values from -0.125 to 0.125
- value_weight: bfloat16 [2048, 2048], P('dp'), may hold values from -0.125 to 0.125
- output_weight: bfloat16 [2048, 2048], P('dp'), may hold values from -0.125 to 0.125
- log_decay: float32 [2, 16], P(None, 'sp'), may hold values from -0.04 to 0, as said below
Outputs:
- mixed: bfloat16 [8, 512, 2048], P('dp', 'sp')
Inputs may be any that keep to these rules, and one draw needn't show every extreme that they name: `log_decay`: every entry is negative: the logarithm of a head's decay per position.
All inputs are finite; a program needn't handle non-finite values.
Results may differ from a plain program's by a relative error of at most 0.012.
Values may be sent and summed in bfloat16 or wider, within the bound.
A program may use at most 128 MiB of HBM per device.

v0:
```python
import jax
import jax.numpy as jnp
from jax import lax
from jax.sharding import PartitionSpec as P

HEADS = 16
DK = 64
DV = 128
BLOCK = 512


exact_precision = lax.Precision.HIGHEST


def rotate(values_part, positions):
    half_dim = values_part.shape[-1] // 2
    frequency = 10000.0 ** (-jnp.arange(half_dim, dtype=jnp.float32) / half_dim)
    angles = positions[:, None] * frequency[None, :]
    cosine = jnp.cos(angles)[:, None, :]
    sine_part = jnp.sin(angles)[:, None, :]
    first = values_part[..., :half_dim]
    second = values_part[..., half_dim:]
    return jnp.concatenate(
        [first * cosine - second * sine_part, first * sine_part + second * cosine], axis=-1
    )


def retain(query, key_rows, value_rows, log_rate):
    length, heads, key_dim = query.shape
    value_dim = value_rows.shape[-1]
    count = length // BLOCK
    offsets = jnp.arange(BLOCK, dtype=jnp.float32)
    distance = offsets[:, None] - offsets[None, :]
    decay_inner = jnp.where(
        distance[None] >= 0.0,
        jnp.exp(log_rate[:, None, None] * jnp.maximum(distance, 0.0)[None]),
        0.0,
    )
    decay_query = jnp.exp((offsets[:, None] + 1.0) * log_rate[None, :])[:, :, None]
    decay_key = jnp.exp((BLOCK - 1.0 - offsets)[:, None] * log_rate[None, :])[:, :, None]
    decay_block = jnp.exp(BLOCK * log_rate)[:, None, None]

    def blocks(array):
        return array.reshape(count, BLOCK, heads, array.shape[-1])

    def advance(state, inputs):
        query_block, key_block, value_block = inputs
        inner = (
            jnp.einsum("ihd,jhd->hij", query_block, key_block, preferred_element_type=jnp.float32)
            * decay_inner
        )
        result = jnp.einsum(
            "hij,jhv->ihv",
            inner.astype(jnp.bfloat16),
            value_block,
            preferred_element_type=jnp.float32,
        )
        query_wide = query_block.astype(jnp.float32) * decay_query
        result = result + jnp.einsum("ihd,hdv->ihv", query_wide, state, precision=exact_precision)
        key_wide = key_block.astype(jnp.float32) * decay_key
        state = state * decay_block + jnp.einsum(
            "jhd,jhv->hdv", key_wide, value_block.astype(jnp.float32), precision=exact_precision
        )
        return (state, result)

    initial = jnp.zeros((heads, key_dim, value_dim), jnp.float32)
    final_state, outputs = lax.scan(
        advance, initial, (blocks(query), blocks(key_rows), blocks(value_rows))
    )
    return outputs.reshape(length, heads, value_dim)


def mechanism(stacked, log_decay):
    length = stacked.shape[0]
    widened = stacked[..., : 2 * DK].astype(jnp.float32)
    positions = jnp.arange(length, dtype=jnp.float32)
    query = rotate(widened[..., :DK], positions).astype(jnp.bfloat16)
    key_rows = rotate(widened[..., DK : 2 * DK], positions).astype(jnp.bfloat16)
    value_rows = stacked[..., 2 * DK :]
    forward = retain(query, key_rows, value_rows, log_decay[0])
    backward = retain(
        jnp.flip(query, 0), jnp.flip(key_rows, 0), jnp.flip(value_rows, 0), log_decay[1]
    )
    combined = forward + jnp.flip(backward, 0)
    average = jnp.mean(combined, axis=-1, keepdims=True)
    centred = combined - average
    variance = jnp.mean(centred * centred, axis=-1, keepdims=True)
    return (centred * lax.rsqrt(variance + 1e-06)).astype(jnp.bfloat16)


def shards(tokens, query_weight, key_weight, value_weight, output_weight, log_decay):
    rows = tokens[0]
    row_count = rows.shape[0]
    local_heads = log_decay.shape[1]
    first_head = lax.axis_index("sp") * local_heads
    own_slices = jnp.concatenate(
        [
            lax.dynamic_slice_in_dim(query_weight, first_head * DK, local_heads * DK, 1),
            lax.dynamic_slice_in_dim(key_weight, first_head * DK, local_heads * DK, 1),
            lax.dynamic_slice_in_dim(value_weight, first_head * DV, local_heads * DV, 1),
        ],
        axis=1,
    )
    own_whole = lax.all_gather(own_slices, "dp", axis=0, tiled=True)
    piece = lax.all_gather(rows, "sp", axis=0, tiled=True)
    count = piece.shape[0]
    product = jnp.dot(piece, own_whole, preferred_element_type=jnp.float32).astype(jnp.bfloat16)
    query_part = product[:, : local_heads * DK].reshape(count, local_heads, DK)
    key_part = product[:, local_heads * DK : 2 * local_heads * DK].reshape(count, local_heads, DK)
    value_part = product[:, 2 * local_heads * DK :].reshape(count, local_heads, DV)
    gathered = jnp.concatenate([query_part, key_part, value_part], axis=2)
    normed = mechanism(gathered, log_decay)
    by_token = lax.all_to_all(normed, "sp", split_axis=0, concat_axis=1, tiled=True).reshape(
        row_count, HEADS * DV
    )
    mixed = jnp.dot(
        by_token,
        lax.all_gather(output_weight, "dp", axis=0, tiled=True),
        preferred_element_type=jnp.float32,
    )
    return mixed.astype(jnp.bfloat16)[None]


def solution(mesh):
    placed = (
        P("dp", "sp", None),
        P("dp", None),
        P("dp", None),
        P("dp", None),
        P("dp", None),
        P(None, "sp"),
    )
    return jax.shard_map(
        shards, mesh=mesh, in_specs=placed, out_specs=P("dp", "sp", None), check_vma=False
    )
```

profile of v0, /device:TPU:0, one launch (start us, length us, event | category | flops | bytes accessed | tf_op | source)
XLA Modules:
  0.0 190.1 jit_solution(7368320106620068643)
XLA Ops:
  6.5 0.7 all-gather.9.cloned.1.call-update
  7.3 0.0 all-gather.5.cloned.1.call-start
  7.3 0.4 copy-done
  7.8 1.0 constant_dynamic-slice_fusion.1
  8.8 0.9 pad_maximum_fusion
  9.7 0.0 all-gather.7.cloned.1.call-start
  9.7 0.7 all-gather.7.cloned.1.call-update
  10.4 1.0 fusion.15
  11.4 0.2 fusion.14
  11.6 0.1 multiply_exponential_fusion.1
  11.7 0.3 fusion.25
  12.0 35.1 %all-gather.9.cloned.1.call-done = bf16[1,512,2048]{2,1,0:T(8,128)(2,1)} async-done(((bf16[1,128,2048]{2,1,0:T(8,128)(2,1)}), bf16[1,512,2048]{2,1,0:T(8,128)(2,1)}) %all-gather.9.cloned.1.call-update) | async-done | bytes 2097168 | tf_op jit(solution)/shard_map/all_gather | solution.py:105
  47.1 48.5 %all-gather.5.cloned.1.call-done = bf16[2048,1024]{1,0:T(8,128)(2,1)} async-done(((bf16[256,1024]{1,0:T(8,128)(2,1)}), bf16[2048,1024]{1,0:T(8,128)(2,1)}) %all-gather.5.cloned.1.call-update) | async-done | bytes 4194320 | tf_op jit(solution)/shard_map/all_gather | solution.py:104
  95.6 5.2 %fusion.8 = bf16[512,1024]{0,1:T(8,128)(2,1)S(1)} fusion(bf16[2048,1024]{1,0:T(8,128)(2,1)} %all-gather.5.cloned.1.call-done, bf16[1,512,2048]{2,1,0:T(8,128)(2,1)} %all-gather.9.cloned.1.call-done), kind=kOutput, calls=%fused_computation.9 | convolution fusion | flops 2148007936 | bytes 7340032 | tf_op jit(solution)/shard_map/dot_general | solution.py:107
  101.0 0.1 maximum_convert_fusion
  101.1 0.2 subtract_convert_fusion
  101.3 1.6 rev.17
  103.0 0.5 rev.16
  103.5 5.7 %rev.15 = bf16[512,4,128]{0,2,1:T(8,128)(2,1)} reverse(bf16[512,4,128]{0,2,1:T(8,128)(2,1)S(1)} %bitcast.36), dimensions={0} | reverse | bytes 1048576 | tf_op jit(solution)/shard_map/jit(_flip)/rev | solution.py:82
  109.2 4.2 %fusion.4 = f32[4,128,512]{2,1,0:T(8,128)} fusion(bf16[512,4,128]{0,2,1:T(8,128)(2,1)} %rev.15, bf16[512,4,64]{0,2,1:T(8,128)(2,1)S(1)} %rev.16, bf16[512,4,64]{0,2,1:T(8,128)(2,1)} %rev.17, f32[4]{0:T(128)} %copy-done.5, f32[512,512]{1,0:T(8,128)S(1)} %fusion.14, pred[512,512]{1,0:T(8,128)(4,1)} %fusion.15), kind=kOutput, calls=%fused_computation.7 | convolution fusion | flops 406847488 | bytes 3407888 | tf_op jit(solution)/shard_map/while/body/eval_jaxpr/hij,jhv->ihv/dot_general | solution.py:52
  113.4 2.2 %fusion.11 = f32[512,4,128]{0,2,1:T(8,128)S(1)} fusion(f32[4,128,512]{2,1,0:T(8,128)} %fusion.4, bf16[512,4,64]{0,2,1:T(8,128)(2,1)S(1)} %rev.16, f32[512,4]{0,1:T(4,128)S(1)} %get-tuple-element.60), kind=kOutput, calls=%fused_computation.11 | convolution fusion | flops 201850880 | bytes 2367488 | tf_op jit(solution)/shard_map/while/body/eval_jaxpr/ihd,hdv->ihv/dot_general | solution.py:59
  115.6 1.5 rev.18
  117.0 3.4 %fusion.3 = f32[4,128,512]{2,1,0:T(8,128)S(1)} fusion(bf16[512,4,128]{0,2,1:T(8,128)(2,1)} %bitcast.37, f32[512,512]{1,0:T(8,128)} %copy-done.2, f32[4]{0:T(128)} %copy-done.4, pred[512,512]{1,0:T(8,128)(4,1)} %fusion.15, bf16[512,4,32]{0,2,1:T(8,128)(2,1)} %copy-done.3, bf16[512,4,32]{0,2,1:T(8,128)(2,1)S(1)} %get-tuple-element.43, ...), kind=kOutput, calls=%fused_computation.6 | convolution fusion | flops 407896064 | bytes 3407888 | tf_op jit(solution)/shard_map/while/body/eval_jaxpr/hij,jhv->ihv/dot_general | solution.py:52
  120.5 1.0 fusion.31
  121.5 0.1 multiply_reduce_fusion
  121.7 0.1 multiply_convert_fusion.2
  121.8 0.3 copy.9
  122.1 12.3 %all_to_all.15 = bf16[512,4,128]{2,1,0:T(4,128)(2,1)S(1)} all-to-all(bf16[512,4,128]{2,1,0:T(4,128)(2,1)S(1)} %copy.9), channel_id=1, replica_groups=mesh['sp'=4,'dp'=8] {'sp'}, dimensions={0} | all-to-all | bytes 1048576 | tf_op jit(solution)/shard_map/all_to_all | solution.py:113
  134.5 0.1 copy.10
  134.6 0.3 copy.11
  134.8 43.3 %all-gather.7.cloned.1.call-done = bf16[2048,2048]{1,0:T(8,128)(2,1)} async-done(((bf16[256,2048]{1,0:T(8,128)(2,1)}), bf16[2048,2048]{1,0:T(8,128)(2,1)}) %all-gather.7.cloned.1.call-update) | async-done | bytes 8388624 | tf_op jit(solution)/shard_map/all_gather | solution.py:118
  178.1 5.5 %fusion = bf16[1,128,2048]{2,1,0:T(8,128)(2,1)} fusion(bf16[128,2048]{0,1:T(8,128)(2,1)S(1)} %bitcast.35, bf16[2048,2048]{1,0:T(8,128)(2,1)} %all-gather.7.cloned.1.call-done), kind=kOutput, calls=%fused_computation.3 | convolution fusion | flops 1074003968 | bytes 9437184 | tf_op jit(solution)/shard_map/dot_general | solution.py:116
  (25 shorter events, 0.2 us)
Async XLA Ops:
  6.5 1.2 copy-start
  6.5 5.0 %copy-start.6 = (f32[2,4]{1,0:T(2,128)S(1)}, f32[2,4]{1,0:T(2,128)}, u32[]{:S(2)}) copy-start(f32[2,4]{1,0:T(2,128)} %param.11) | copy-start | bytes 100
  6.5 40.6 %all-gather.9.cloned.1.call-start = ((), (), s32[]{:S(2)}) async-start(), calls=%async_computation.3 | async-start | bytes 2621440 | tf_op jit(solution)/shard_map/all_gather | solution.py:105
  7.3 88.3 %all-gather.5.cloned.1.call-start = ((), (), s32[]{:S(2)}) async-start(), calls=%async_computation.1 | async-start | bytes 4718592 | tf_op jit(solution)/shard_map/all_gather | solution.py:104
  9.7 168.5 %all-gather.7.cloned.1.call-start = ((), (), s32[]{:S(2)}) async-start(), calls=%async_computation.2 | async-start | bytes 9437184 | tf_op jit(solution)/shard_map/all_gather | solution.py:118
  11.6 97.6 %copy-start.2 = (f32[512,512]{1,0:T(8,128)}, f32[512,512]{1,0:T(8,128)S(1)}, u32[]{:S(2)}) copy-start(f32[512,512]{1,0:T(8,128)S(1)} %fusion.14) | copy-start | bytes 3145732
  11.6 89.3 %copy-start.4 = (f32[4]{0:T(128)}, f32[4]{0:T(128)S(1)}, u32[]{:S(2)}) copy-start(f32[4]{0:T(128)S(1)} %get-tuple-element.61) | copy-start | bytes 52
  11.6 89.3 %copy-start.5 = (f32[4]{0:T(128)}, f32[4]{0:T(128)S(1)}, u32[]{:S(2)}) copy-start(f32[4]{0:T(128)S(1)} %get-tuple-element.62) | copy-start | bytes 52
  100.9 12.4 %copy-start.1 = (bf16[512,512]{0,1:T(8,128)(2,1)}, bf16[512,512]{0,1:T(8,128)(2,1)S(1)}, u32[]{:S(2)}) copy-start(bf16[512,512]{0,1:T(8,128)(2,1)S(1)} %slice.42) | copy-start | bytes 1572868
  101.3 1.7 copy-start.3
Sparse Core Ops, SparseCore 0:
  9.2 37.8 all-gather.8
  48.7 46.8 all-gather.4
  97.2 80.8 all-gather.6
where the time goes:
time: 190 us
  waiting for transfers between devices  128 us (67%)
  matrix products  21.5 us (11%)
  between operations  13.3 us (7%)
  blocking collectives  12.3 us (6%)
  local copies, waits for them, and re-layouts  11.6 us (6%)
  other arithmetic  3.01 us (2%)
    all_gather x1, waiting for transfers between devices, shards(): own_whole = lax.all_gather(own_slices, 'dp', axis=0, tiled=True)  48.5 us
    all_gather x1, waiting for transfers between devices, shards(): lax.all_gather(output_weight, 'dp', axis=0, tiled=True)  43.3 us
    all_gather x1, waiting for transfers between devices, shards(): piece = lax.all_gather(rows, 'sp', axis=0, tiled=True)  35.1 us
    all_to_all x1, blocking collectives, shards(): lax.all_to_all(normed, 'sp', split_axis=0, concat_axis=1, tiled=True)  12.3 us
    dot_general x2, matrix products, advance(): jnp.einsum('hij,jhv->ihv', inner.astype(jnp.bfloat16), value_block, prefe...  7.56 us
    rev x1, local copies, waits for them, and re-layouts, mechanism(): jnp.flip(value_rows, 0)  5.71 us
    dot_general x1, matrix products, shards(): jnp.dot(by_token, lax.all_gather(output_weight, 'dp', axis=0, tiled=True)...  5.46 us
    dot_general x1, matrix products, shards(): jnp.dot(piece, own_whole, preferred_element_type=jnp.float32)  5.25 us
  transfers between devices with their start and end apart: 3, of which 3 were waited for; matrix products, arithmetic and copies ran while one was open for 16% of the time, Pallas kernels for 0%

commit v1 on v0

--- a/solution.py
+++ b/solution.py
@@ -1,6 +1,11 @@
+import functools
+
+import numpy as np
 import jax
 import jax.numpy as jnp
 from jax import lax
+from jax.experimental import pallas as pl
+from jax.experimental.pallas import tpu as pltpu
 from jax.sharding import PartitionSpec as P
 
 HEADS = 16
@@ -121,7 +126,390 @@
     return mixed.astype(jnp.bfloat16)[None]
 
 
+MESH = pl.DeviceIdType.MESH
+CORES = 2
+PIECES = 2
+
+
+def tables(length):
+    half = DK // 2
+    frequency = (10000.0 ** (-np.arange(half) / half)).astype(np.float32)
+    angles = (np.arange(length, dtype=np.float32)[:, None] * frequency[None, :]).astype(np.float64)
+    cosine = np.tile(np.cos(angles), (1, 4)).astype(np.float32)
+    sine = np.tile(np.sin(angles), (1, 4)).astype(np.float32)
+    swap = np.zeros((2 * DK, 2 * DK), np.float32)
+    for lane in range(2 * DK):
+        if lane % DK < half:
+            swap[lane + half, lane] = -1.0
+        else:
+            swap[lane - half, lane] = 1.0
+    return jnp.asarray(cosine), jnp.asarray(sine), jnp.asarray(swap, jnp.bfloat16)
+
+
+def layer_kernel(
+    S, Z, rate_ref, cos_ref, sin_ref, swap_ref, x_ref, wq_ref, wk_ref, wv_ref, wo_ref, out_ref,
+    tok, wqkv, wo, acc, decay, qk, val, nsend, nrm, oacc,
+    lsem, tS, tR, qS, qR, qpS, qpR, oS, oR, iS, iR, dS, dR, opS, opR, nS, nR,
+):
+    s = lax.axis_index("sp")
+    d = lax.axis_index("dp")
+    z, c = d // CORES, d % CORES
+    rows, model = x_ref.shape
+    length = S * rows
+    depth = wq_ref.shape[0]
+    heads = rate_ref.shape[1]
+    qc, vc = heads * DK, heads * DV
+    oc = wo.shape[3]
+    step_rows = depth // PIECES
+    sx = s + 1 - 2 * (s % 2)
+    sy = (s + 2) % 4
+    sd = (sx + 2) % 4
+    partner = {"dp": z * CORES + 1 - c}
+
+    def remote(src, send, recv, device, dst=None):
+        return pltpu.make_async_remote_copy(
+            src_ref=src, dst_ref=src if dst is None else dst, send_sem=send, recv_sem=recv,
+            device_id=device, device_id_type=MESH,
+        )
+
+    local = [
+        pltpu.make_async_copy(wq_ref.at[:, pl.ds(pl.multiple_of(s * qc, qc), qc)], wqkv.at[d, :, pl.ds(0, qc)], lsem.at[0]),
+        pltpu.make_async_copy(wk_ref.at[:, pl.ds(pl.multiple_of(s * qc, qc), qc)], wqkv.at[d, :, pl.ds(qc, qc)], lsem.at[1]),
+        pltpu.make_async_copy(wv_ref.at[:, pl.ds(pl.multiple_of(s * vc, vc), vc)], wqkv.at[d, :, pl.ds(2 * qc, vc)], lsem.at[2]),
+        pltpu.make_async_copy(x_ref, tok.at[s], lsem.at[3]),
+    ] + [
+        pltpu.make_async_copy(wo_ref.at[:, pl.ds(j * oc, oc)], wo.at[d, j], lsem.at[4 + j]) for j in range(S)
+    ]
+    for copy in local:
+        copy.start()
+
+    barrier = pltpu.get_barrier_semaphore()
+
+    def greet(device):
+        pl.semaphore_signal(barrier, inc=1, device_id=device, device_id_type=MESH)
+
+    for other in range(1, S):
+        greet({"sp": (s + other) % S})
+    greet(partner)
+    pl.when(z > 0)(lambda: greet({"dp": d - CORES}))
+    pl.when(z < Z - 1)(lambda: greet({"dp": d + CORES}))
+    inside = (z > 0) & (z < Z - 1)
+    pl.when(inside)(lambda: pl.semaphore_wait(barrier, S + 2))
+    pl.when(jnp.logical_not(inside))(lambda: pl.semaphore_wait(barrier, S + min(Z - 1, 1)))
+
+    def side(way):
+        return {"dp": d + CORES if way == 0 else d - CORES}
+
+    def has_side(way):
+        return z < Z - 1 if way == 0 else z > 0
+
+    def q_copy(way, src, piece, to=None):
+        ref = wqkv.at[src * CORES + c, pl.ds(piece * step_rows, step_rows)]
+        return remote(ref, qS.at[way, src, piece], qR.at[src, piece], side(way if to is None else to))
+
+    def o_piece(block, quarter, piece):
+        return wo.at[block, quarter, pl.ds(piece * step_rows, step_rows)]
+
+    def o_copy(way, src, piece, to=None):
+        return remote(o_piece(src * CORES + c, s, piece), oS.at[way, src, piece], oR.at[src, piece], side(way if to is None else to))
+
+    def qp_copy(src, mine=True):
+        ref = wqkv.at[src * CORES + (c if mine else 1 - c)]
+        return remote(ref, qpS.at[src], qpR.at[src], partner)
+
+    def op_copy(src, mine=True):
+        ref = wo.at[src * CORES + (c if mine else 1 - c)]
+        return remote(ref, opS.at[src], opR.at[src], partner)
+
+    def i_copy(axis, src, piece, mine=True):
+        to = sx if axis == 0 else sy
+        return remote(o_piece(src * CORES + c, s if mine else to, piece), iS.at[axis, src, piece], iR.at[axis, src, piece], {"sp": to})
+
+    def d_copy(src, piece, mine=True):
+        first = piece < PIECES // 2
+        to = sy if first else sx
+        quarter = (sx if first else sy) if mine else sd
+        return remote(o_piece(src * CORES + c, quarter, piece), dS.at[src, piece], dR.at[src, piece], {"sp": to})
+
+    def t_copy(other):
+        to = (s + other) % S
+        return remote(tok.at[s], tS.at[other], tR.at[other], {"sp": to})
+
+    def t_wait(other):
+        frm = (s + S - other) % S
+        remote(tok.at[frm], tS.at[other], tR.at[other], {"sp": frm}).wait_recv()
+
+    def n_copy(head, j):
+        return remote(
+            nsend.at[head, j], nS.at[head, j], nR.at[head, s], {"sp": j},
+            dst=nrm.at[s, :, pl.ds(head * DV, DV)],
+        )
+
+    def n_wait(head, j):
+        remote(nsend.at[head, j], nS.at[head, j], nR.at[head, j], {"sp": j}, dst=nrm.at[j, :, pl.ds(head * DV, DV)]).wait_recv()
+
+    def each(count, fn):
+        for piece in range(count):
+            fn(piece)
+
+    def own_o(way):
+        each(PIECES, lambda piece: o_copy(way, z, piece).start())
+
+    for copy in local[:3]:
+        copy.wait()
+    for way in (0, 1):
+        pl.when(has_side(way))(lambda way=way: each(PIECES, lambda piece: q_copy(way, z, piece).start()))
+    local[3].wait()
+    for other in range(1, S):
+        t_copy(other).start()
+    qp_copy(z).start()
+    for copy in local[4:]:
+        copy.wait()
+    op_copy(z).start()
+    pl.when(z == 0)(lambda: own_o(0))
+    pl.when(z == Z - 1)(lambda: own_o(1))
+
+    for head in range(heads):
+        fast, slow = rate_ref[0, head], rate_ref[1, head]
+
+        @pl.loop(0, S)
+        def _(j):
+            at = lax.broadcasted_iota(jnp.int32, (rows, length), 0) + j * rows
+            gap = (at - lax.broadcasted_iota(jnp.int32, (rows, length), 1)).astype(jnp.float32)
+            weight = jnp.exp(jnp.where(gap >= 0.0, gap * fast, gap * (-slow)))
+            decay[head, pl.ds(pl.multiple_of(j * rows, rows), rows), :] = jnp.where(gap == 0.0, 2.0, weight)
+
+    width = 2 * qc + vc
+    tile = 256
+
+    def project(src, first):
+        qp_copy(src, mine=False).wait_recv()
+        wide = CORES * depth
+        cols = pl.ds(pl.multiple_of(src * wide, wide), wide)
+
+        @pl.loop(0, width // tile)
+        def _(n):
+            at = pl.ds(pl.multiple_of(n * tile, tile), tile)
+            part = jnp.dot(
+                tok[:, :, cols].reshape(length, wide),
+                wqkv[pl.ds(src * CORES, CORES), :, at].reshape(wide, tile),
+                preferred_element_type=jnp.float32,
+            )
+            if first:
+                acc[:, at] = part
+            else:
+                acc[:, at] += part
+
+    for other in range(1, S):
+        t_wait(other)
+    project(z, True)
+
+    def sources(k):
+        return ((0, z - k, z - k >= 0), (1, z + k, z + k < Z))
+
+    for k in range(1, Z):
+        for way, src, there in sources(k):
+            @pl.when(there)
+            def _():
+                for piece in range(PIECES):
+                    q_copy(way, src, piece, 1 - way).wait_recv()
+                    pl.when(has_side(way))(lambda: q_copy(way, src, piece).start())
+                qp_copy(src).start()
+        if k < Z - 1:
+            pl.when(z == k)(lambda: own_o(0))
+            pl.when(z == Z - 1 - k)(lambda: own_o(1))
+        for way, src, there in sources(k):
+            pl.when(there)(lambda: project(src, False))
+
+    for pair in range(qc // (2 * DK)):
+        for part in range(2):
+            at = pl.ds(part * qc + pair * 2 * DK, 2 * DK)
+            flat = acc[:, at].astype(jnp.bfloat16)
+            turned = jnp.dot(flat, swap_ref[...], preferred_element_type=jnp.float32)
+            qk[:, at] = (flat.astype(jnp.float32) * cos_ref[...] + turned * sin_ref[...]).astype(jnp.bfloat16)
+    val[...] = acc[:, 2 * qc :].astype(jnp.bfloat16)
+
+    def retain_head(head):
+        pair = head // 2
+        lane = lax.broadcasted_iota(jnp.int32, (rows, 2 * DK), 1)
+        mine = (lane // DK) == (head % 2)
+        for j in range(S):
+            here = slice(j * rows, (j + 1) * rows)
+            query = qk[here, pair * 2 * DK : (pair + 1) * 2 * DK]
+            query = jnp.where(mine, query.astype(jnp.float32), 0.0).astype(jnp.bfloat16)
+            scores = lax.dot_general(
+                query, qk[:, qc + pair * 2 * DK : qc + (pair + 1) * 2 * DK],
+                (((1,), (1,)), ((), ())), preferred_element_type=jnp.float32,
+            )
+            scores = (scores * decay[head, here, :]).astype(jnp.bfloat16)
+            ret = jnp.dot(scores, val[:, head * DV : (head + 1) * DV], preferred_element_type=jnp.float32)
+            centred = ret - jnp.mean(ret, axis=-1, keepdims=True)
+            variance = jnp.mean(centred * centred, axis=-1, keepdims=True)
+            normed = (centred * lax.rsqrt(variance + 1e-06)).astype(jnp.bfloat16)
+            nsend[head, j] = normed
+
+            @pl.when(j == s)
+            def _():
+                nrm[s, :, head * DV : (head + 1) * DV] = normed
+
+            @pl.when(j != s)
+            def _():
+                n_copy(head, j).start()
+
+    def o_step(k):
+        for way, src, there in sources(k):
+            @pl.when(there)
+            def _():
+                for piece in range(PIECES):
+                    o_copy(way, src, piece, 1 - way).wait_recv()
+                    pl.when(has_side(way))(lambda: o_copy(way, src, piece).start())
+                    i_copy(0, src, piece).start()
+                    i_copy(1, src, piece).start()
+
+    def o_relay(k):
+        for way, src, there in sources(k):
+            @pl.when(there)
+            def _():
+                for piece in range(PIECES):
+                    i_copy(0, src, piece, mine=False).wait_recv()
+                    i_copy(1, src, piece, mine=False).wait_recv()
+                    d_copy(src, piece).start()
+
+    def o_share(k):
+        for way, src, there in sources(k):
+            @pl.when(there)
+            def _():
+                for piece in range(PIECES):
+                    d_copy(src, piece, mine=False).wait_recv()
+                op_copy(src).start()
+
+    def finish(src, first):
+        op_copy(src, mine=False).wait_recv()
+
+        @pl.loop(0, S)
+        def _(j):
+            at = pl.ds(pl.multiple_of(j * oc, oc), oc)
+            part = jnp.dot(
+                nrm[src], wo[pl.ds(src * CORES, CORES), j].reshape(CORES * depth, oc),
+                preferred_element_type=jnp.float32,
+            )
+            if first:
+                oacc[:, at] = part
+            else:
+                oacc[:, at] += part
+
+    for head in range(heads):
+        retain_head(head)
+        if head == heads - 2:
+            o_step(1)
+    o_step(2)
+    o_relay(1)
+    for j in range(S):
+        @pl.when(j != s)
+        def _():
+            for head in range(heads):
+                n_wait(head, j)
+    finish(z, True)
+    o_share(1)
+    o_step(3)
+    o_relay(2)
+    for way, src, there in sources(1):
+        pl.when(there)(lambda: finish(src, False))
+    o_share(2)
+    o_relay(3)
+    for way, src, there in sources(2):
+        pl.when(there)(lambda: finish(src, False))
+    o_share(3)
+    for way, src, there in sources(3):
+        pl.when(there)(lambda: finish(src, False))
+    out_ref[...] = oacc[...].astype(out_ref.dtype)
+
+    for other in range(1, S):
+        t_copy(other).wait_send()
+    for way in (0, 1):
+        @pl.when(has_side(way))
+        def _():
+            for piece in range(PIECES):
+                q_copy(way, z, piece).wait_send()
+                o_copy(way, z, piece).wait_send()
+    qp_copy(z).wait_send()
+    op_copy(z).wait_send()
+    for k in range(1, Z):
+        for way, src, there in sources(k):
+            @pl.when(there)
+            def _():
+                qp_copy(src).wait_send()
+                op_copy(src).wait_send()
+                for piece in range(PIECES):
+                    i_copy(0, src, piece).wait_send()
+                    i_copy(1, src, piece).wait_send()
+                    d_copy(src, piece).wait_send()
+
+            @pl.when(there & has_side(way))
+            def _():
+                for piece in range(PIECES):
+                    q_copy(way, src, piece).wait_send()
+                    o_copy(way, src, piece).wait_send()
+    for head in range(heads):
+        for j in range(S):
+            pl.when(j != s)(lambda: n_copy(head, j).wait_send())
+
+
+def fused(S, Z, tokens, query_weight, key_weight, value_weight, output_weight, log_decay):
+    rows, model = tokens.shape[1:]
+    depth = query_weight.shape[0]
+    heads = log_decay.shape[1]
+    length = S * rows
+    width = heads * (2 * DK + DV)
+    oc = output_weight.shape[1] // S
+    cosine, sine, swap = tables(length)
+    vmem, anyplace = pl.BlockSpec(memory_space=pltpu.VMEM), pl.BlockSpec(memory_space=pl.ANY)
+    dma = pltpu.SemaphoreType.DMA
+    bf, f32 = jnp.bfloat16, jnp.float32
+    out = pl.pallas_call(
+        functools.partial(layer_kernel, S, Z),
+        out_shape=jax.ShapeDtypeStruct((rows, output_weight.shape[1]), bf),
+        in_specs=[pl.BlockSpec(memory_space=pltpu.SMEM)] + [vmem] * 3 + [anyplace] * 5,
+        out_specs=vmem,
+        scratch_shapes=[
+            pltpu.VMEM((S, rows, model), bf),
+            pltpu.VMEM((Z * CORES, depth, width), bf),
+            pltpu.VMEM((Z * CORES, S, depth, oc), bf),
+            pltpu.VMEM((length, width), f32),
+            pltpu.VMEM((heads, length, length), f32),
+            pltpu.VMEM((length, 2 * heads * DK), bf),
+            pltpu.VMEM((length, heads * DV), bf),
+            pltpu.VMEM((heads, S, rows, DV), bf),
+            pltpu.VMEM((S, rows, heads * DV), bf),
+            pltpu.VMEM((rows, S * oc), f32),
+            dma((4 + S,)), dma((S,)), dma((S,)),
+            dma((2, Z, PIECES)), dma((Z, PIECES)), dma((Z,)), dma((Z,)),
+            dma((2, Z, PIECES)), dma((Z, PIECES)),
+            dma((2, Z, PIECES)), dma((2, Z, PIECES)), dma((Z, PIECES)), dma((Z, PIECES)),
+            dma((Z,)), dma((Z,)), dma((heads, S)), dma((heads, S)),
+        ],
+        compiler_params=pltpu.CompilerParams(
+            collective_id=0, has_side_effects=True, vmem_limit_bytes=60 * 1024 * 1024
+        ),
+    )(log_decay, cosine, sine, swap, tokens[0], query_weight, key_weight, value_weight, output_weight)
+    return out[None]
+
+
 def solution(mesh):
+    S, D = mesh.shape["sp"], mesh.shape["dp"]
+    Z = D // CORES
+
+    def layer(tokens, query_weight, key_weight, value_weight, output_weight, log_decay):
+        rows = tokens.shape[1]
+        depth = query_weight.shape[0]
+        heads = log_decay.shape[1]
+        fits = (
+            S == 4 and D == CORES * Z and S * rows == BLOCK and (heads * DK) % 256 == 0
+            and heads * DV == CORES * depth and rows % 128 == 0
+        )
+        args = (tokens, query_weight, key_weight, value_weight, output_weight, log_decay)
+        return fused(S, Z, *args) if fits else shards(*args)
+
     placed = (
         P("dp", "sp", None),
         P("dp", None),
@@ -131,5 +519,5 @@
         P(None, "sp"),
     )
     return jax.shard_map(
-        shards, mesh=mesh, in_specs=placed, out_specs=P("dp", "sp", None), check_vma=False
-    )
+        layer, mesh=mesh, in_specs=placed, out_specs=P("dp", "sp", None), check_vma=False
+    )

time: 190 us -> 105 us (0.55)
  waiting for transfers between devices: 128 us -> 0 us
  Pallas kernels: 0 us -> 103 us
  matrix products: 21.5 us -> 0 us
  between operations: 13.3 us -> 0.01 us
  blocking collectives: 12.3 us -> 0 us
  local copies, waits for them, and re-layouts: 11.6 us -> 1.88 us
  other arithmetic: 3.01 us -> 0 us
    all_gather x3 -> x0, waiting for transfers between devices: 127 us -> none  [the longest x1 48.5 us: shards(): own_whole = lax.all_gather(own_slices, 'dp', axis=0, tiled=True)]
    pallas_call x0 -> x1, Pallas kernels: none -> 103 us  [fused(): pl.pallas_call(functools.partial(layer_kernel, S, Z), out_shape=jax.Shape...]
    dot_general x6 -> x0, matrix products: 21.5 us -> none  [the longest x2 7.56 us: advance(): jnp.einsum('hij,jhv->ihv', inner.astype(jnp.bfloat16), value_block, prefe...]
    all_to_all x1 -> x0, blocking collectives: 12.3 us -> none  [shards(): lax.all_to_all(normed, 'sp', split_axis=0, concat_axis=1, tiled=True)]
    rev x4 -> x0, local copies, waits for them, and re-layouts: 9.34 us -> none  [the longest x1 5.71 us: mechanism(): jnp.flip(value_rows, 0)]
  transfers between devices with their start and end apart: 3 -> 0, of which waited for: 3 -> 0; matrix products, arithmetic and copies ran while one was open for 16% -> 0% of each run, Pallas kernels for 0% -> 0%
where the time goes in v1:
time: 105 us
  Pallas kernels  103 us (98%)
  local copies, waits for them, and re-layouts  1.88 us (2%)
    pallas_call x1, Pallas kernels, fused(): pl.pallas_call(functools.partial(layer_kernel, S, Z), out_shape=jax.Shape...  103 us

profile of v1, /device:TPU:0, one launch (start us, length us, event | category | flops | bytes accessed | tf_op | source)
XLA Modules:
  0.0 104.5 jit_solution(3404120017324428044)
XLA Ops:
  0.0 102.6 %shard_map.91 = bf16[128,2048]{1,0:T(8,128)(2,1)} custom-call(f32[2,4]{1,0:T(2,128)} %rate_ref.1, f32[512,128]{1,0:T(8,128)} %constant.6.clone.cos_ref, f32[512,128]{1,0:T(8,128)} %constant.7.clone.sin_ref, bf16[128,128]{1,0:T(8,128)(2,1)} %constant.8.clone.swap_ref, bf16[128,2048]{1,0:T(8,128)(2,1)} %bitcast.3, bf16[256,1024]{1,0:T(8,128)(2,1)} %wq_ref.1, ...), custom_call_target="tpu_custom_call" | custom-call | tf_op jit(solution)/shard_map/pallas_call | solution.py:469
  102.6 1.9 %copy.11 = bf16[1,128,2048]{2,1,0:T(8,128)(2,1)} copy(bf16[1,128,2048]{2,1,0:T(8,128)(2,1)} %bitcast.2) | data formatting | bytes 1048576

commit v2 on v1

--- a/solution.py
+++ b/solution.py
@@ -265,9 +265,9 @@
     qp_copy(z).start()
     for copy in local[4:]:
         copy.wait()
+    for way in (0, 1):
+        pl.when(has_side(way))(lambda way=way: own_o(way))
     op_copy(z).start()
-    pl.when(z == 0)(lambda: own_o(0))
-    pl.when(z == Z - 1)(lambda: own_o(1))
 
     for head in range(heads):
         fast, slow = rate_ref[0, head], rate_ref[1, head]
@@ -307,7 +307,7 @@
     def sources(k):
         return ((0, z - k, z - k >= 0), (1, z + k, z + k < Z))
 
-    for k in range(1, Z):
+    def q_step(k):
         for way, src, there in sources(k):
             @pl.when(there)
             def _():
@@ -315,11 +315,51 @@
                     q_copy(way, src, piece, 1 - way).wait_recv()
                     pl.when(has_side(way))(lambda: q_copy(way, src, piece).start())
                 qp_copy(src).start()
-        if k < Z - 1:
-            pl.when(z == k)(lambda: own_o(0))
-            pl.when(z == Z - 1 - k)(lambda: own_o(1))
+
+    def o_step(k):
+        for way, src, there in sources(k):
+            @pl.when(there)
+            def _():
+                for piece in range(PIECES):
+                    o_copy(way, src, piece, 1 - way).wait_recv()
+                    pl.when(has_side(way))(lambda: o_copy(way, src, piece).start())
+                for piece in range(PIECES):
+                    i_copy(0, src, piece).start()
+                    i_copy(1, src, PIECES - 1 - piece).start()
+
+    def o_relay(k):
+        for way, src, there in sources(k):
+            @pl.when(there)
+            def _():
+                for near in range(PIECES // 2):
+                    for axis, piece in ((0, near), (1, PIECES - 1 - near)):
+                        i_copy(axis, src, piece, mine=False).wait_recv()
+                        d_copy(src, piece).start()
+
+    def o_share(k):
+        for way, src, there in sources(k):
+            @pl.when(there)
+            def _():
+                for near in range(PIECES // 2):
+                    i_copy(1, src, near, mine=False).wait_recv()
+                    i_copy(0, src, PIECES - 1 - near, mine=False).wait_recv()
+                for piece in range(PIECES):
+                    d_copy(src, piece, mine=False).wait_recv()
+                op_copy(src).start()
+
+    def project_step(k):
         for way, src, there in sources(k):
             pl.when(there)(lambda: project(src, False))
+
+    q_step(1)
+    o_step(1)
+    project_step(1)
+    q_step(2)
+    o_step(2)
+    o_relay(1)
+    project_step(2)
+    q_step(3)
+    project_step(3)
 
     for pair in range(qc // (2 * DK)):
         for part in range(2):
@@ -356,33 +396,6 @@
             def _():
                 n_copy(head, j).start()
 
-    def o_step(k):
-        for way, src, there in sources(k):
-            @pl.when(there)
-            def _():
-                for piece in range(PIECES):
-                    o_copy(way, src, piece, 1 - way).wait_recv()
-                    pl.when(has_side(way))(lambda: o_copy(way, src, piece).start())
-                    i_copy(0, src, piece).start()
-                    i_copy(1, src, piece).start()
-
-    def o_relay(k):
-        for way, src, there in sources(k):
-            @pl.when(there)
-            def _():
-                for piece in range(PIECES):
-                    i_copy(0, src, piece, mine=False).wait_recv()
-                    i_copy(1, src, piece, mine=False).wait_recv()
-                    d_copy(src, piece).start()
-
-    def o_share(k):
-        for way, src, there in sources(k):
-            @pl.when(there)
-            def _():
-                for piece in range(PIECES):
-                    d_copy(src, piece, mine=False).wait_recv()
-                op_copy(src).start()
-
     def finish(src, first):
         op_copy(src, mine=False).wait_recv()
 
@@ -398,30 +411,29 @@
             else:
                 oacc[:, at] += part
 
+    def finish_step(k):
+        for way, src, there in sources(k):
+            pl.when(there)(lambda: finish(src, False))
+
     for head in range(heads):
         retain_head(head)
+        if head == 0:
+            o_relay(2)
         if head == heads - 2:
-            o_step(1)
-    o_step(2)
-    o_relay(1)
+            o_step(3)
+    o_share(1)
+    o_relay(3)
     for j in range(S):
         @pl.when(j != s)
         def _():
             for head in range(heads):
                 n_wait(head, j)
     finish(z, True)
-    o_share(1)
-    o_step(3)
-    o_relay(2)
-    for way, src, there in sources(1):
-        pl.when(there)(lambda: finish(src, False))
+    finish_step(1)
     o_share(2)
-    o_relay(3)
-    for way, src, there in sources(2):
-        pl.when(there)(lambda: finish(src, False))
     o_share(3)
-    for way, src, there in sources(3):
-        pl.when(there)(lambda: finish(src, False))
+    finish_step(2)
+    finish_step(3)
     out_ref[...] = oacc[...].astype(out_ref.dtype)
 
     for other in range(1, S):

time: 105 us -> 92.4 us (0.88)
  Pallas kernels: 103 us -> 90.4 us
    pallas_call x1, Pallas kernels: 103 us -> 90.4 us  [fused(): pl.pallas_call(functools.partial(layer_kernel, S, Z), out_shape=jax.Shape...]
where the time goes in v2:
time: 92.4 us; the launch traced here: 92.3 us
  Pallas kernels  90.4 us (98%)
  local copies, waits for them, and re-layouts  1.88 us (2%)
    pallas_call x1, Pallas kernels, fused(): pl.pallas_call(functools.partial(layer_kernel, S, Z), out_shape=jax.Shape...  90.4 us
    unnamed x1, local copies, waits for them, and re-layouts  1.88 us

profile of v2, /device:TPU:0, one launch (start us, length us, event | category | flops | bytes accessed | tf_op | source)
XLA Modules:
  0.0 92.3 jit_solution(2830440097022875154)
XLA Ops:
  0.0 90.4 %shard_map.91 = bf16[128,2048]{1,0:T(8,128)(2,1)} custom-call(f32[2,4]{1,0:T(2,128)} %rate_ref.1, f32[512,128]{1,0:T(8,128)} %constant.6.clone.cos_ref, f32[512,128]{1,0:T(8,128)} %constant.7.clone.sin_ref, bf16[128,128]{1,0:T(8,128)(2,1)} %constant.8.clone.swap_ref, bf16[128,2048]{1,0:T(8,128)(2,1)} %bitcast.3, bf16[256,1024]{1,0:T(8,128)(2,1)} %wq_ref.1, ...), custom_call_target="tpu_custom_call" | custom-call | tf_op jit(solution)/shard_map/pallas_call | solution.py:481
  90.4 1.9 %copy.11 = bf16[1,128,2048]{2,1,0:T(8,128)(2,1)} copy(bf16[1,128,2048]{2,1,0:T(8,128)(2,1)} %bitcast.2) | data formatting | bytes 1048576

commit v3 on v2

--- a/solution.py
+++ b/solution.py
@@ -300,10 +300,6 @@
             else:
                 acc[:, at] += part
 
-    for other in range(1, S):
-        t_wait(other)
-    project(z, True)
-
     def sources(k):
         return ((0, z - k, z - k >= 0), (1, z + k, z + k < Z))
 
@@ -353,6 +349,9 @@
 
     q_step(1)
     o_step(1)
+    for other in range(1, S):
+        t_wait(other)
+    project(z, True)
     project_step(1)
     q_step(2)
     o_step(2)

time: 92.4 us -> 83.8 us (0.907)
  Pallas kernels: 90.4 us -> 81.8 us
    pallas_call x1, Pallas kernels: 90.4 us -> 81.8 us  [fused(): pl.pallas_call(functools.partial(layer_kernel, S, Z), out_shape=jax.Shape...]
where the time goes in v3:
time: 83.8 us; the launch traced here: 83.7 us
  Pallas kernels  81.8 us (98%)
  local copies, waits for them, and re-layouts  1.88 us (2%)
    pallas_call x1, Pallas kernels, fused(): pl.pallas_call(functools.partial(layer_kernel, S, Z), out_shape=jax.Shape...  81.8 us
    unnamed x1, local copies, waits for them, and re-layouts  1.88 us

profile of v3, /device:TPU:0, one launch (start us, length us, event | category | flops | bytes accessed | tf_op | source)
XLA Modules:
  0.0 83.7 jit_solution(9006753730702439923)
XLA Ops:
  0.0 81.8 %shard_map.91 = bf16[128,2048]{1,0:T(8,128)(2,1)} custom-call(f32[2,4]{1,0:T(2,128)} %rate_ref.1, f32[512,128]{1,0:T(8,128)} %constant.6.clone.cos_ref, f32[512,128]{1,0:T(8,128)} %constant.7.clone.sin_ref, bf16[128,128]{1,0:T(8,128)(2,1)} %constant.8.clone.swap_ref, bf16[128,2048]{1,0:T(8,128)(2,1)} %bitcast.3, bf16[256,1024]{1,0:T(8,128)(2,1)} %wq_ref.1, ...), custom_call_target="tpu_custom_call" | custom-call | tf_op jit(solution)/shard_map/pallas_call | solution.py:480
  81.8 1.9 %copy.11 = bf16[1,128,2048]{2,1,0:T(8,128)(2,1)} copy(bf16[1,128,2048]{2,1,0:T(8,128)(2,1)} %bitcast.2) | data formatting | bytes 1048576
